TPU v7x, 128 devices: a whole 4x4x4 slice. The times are simulated.
128 devices in a mesh: ra: 16 (over z, x), cb: 8 (over y, core).
Axes of the slice: x: 4, y: 4, z: 4, core: 2. Of those that a mesh axis runs over, the one named last changes fastest.
Arguments:
- inputs: bfloat16 [1536, 4096], P(None, 'ra'), may hold values from -12 to 12
- gate_weight: bfloat16 [2, 4096, 11264], P(None, 'ra', 'cb'), may hold values from -0.09375 to 0.09375
- up_weight: bfloat16 [2, 4096, 11264], P(None, 'ra', 'cb'), may hold values from -0.09375 to 0.09375
- down_weight: bfloat16 [2, 11264, 4096], P(None, 'cb', 'ra'), may hold values from -0.0546875 to 0.0546875
- norm_gain: float32 [2, 4096], P(None, 'ra'), may hold values from 0.05 to 8
- norm_shift: float32 [2, 4096], P(None, 'ra'), may hold values from -1.5 to 1.5
Outputs:
- outputs: bfloat16 [1536, 4096], P(None, 'ra')
All inputs are finite; a program needn't handle non-finite values.
Results may differ from a plain program's by a relative error of at most 0.04.
Values may be sent and summed in bfloat16 or wider, within the bound.
No kernel may reach another device: no remote copies, remote signals or barrier semaphores. Data moves between devices by JAX's collectives and lax.ppermute only.
A program may use at most 64 MiB of HBM per device.

v0:
```python
import jax
import jax.numpy as jnp
from jax import lax
from jax.sharding import Mesh
from jax.sharding import PartitionSpec as P

RESIDUAL = 0.5
EPSILON = 1e-05
BF16 = jnp.bfloat16
F32 = jnp.float32


def exchange(parts, axes):
    return lax.all_to_all(parts, axes, 0, 0, tiled=True)


def share(block, axes, peers):
    return exchange(jnp.broadcast_to(block[None], (peers, *block.shape)), axes)


def swap_core(block):
    return lax.ppermute(block, "c", [(0, 1), (1, 0)])


def dot_nt(a, b):
    return lax.dot_general(a, b, (((1,), (1,)), ((), ())), preferred_element_type=F32)


def regroup_weights(gate, up, down):
    stacked = jnp.stack((gate.T, up.T, down))
    rows = stacked.shape[1] // 4
    parts = stacked.reshape(3, 4, rows, 256).transpose(1, 0, 2, 3)
    mine = exchange(parts, "x")
    mine = mine.transpose(1, 2, 0, 3).reshape(3, rows, 1024)
    other = swap_core(mine)
    both = jnp.concatenate((mine, other), axis=1)
    return (both[:2].reshape(2 * 2 * rows, 1024), both[2])


def normed(mixed, row_sum, row_squares, gain, shift):
    mean = row_sum / 4096.0
    var = row_squares / 4096.0 - mean * mean
    out = (mixed - mean[:, None]) * lax.rsqrt(var + EPSILON)[:, None]
    return (out * gain + shift).astype(BF16)


def hidden_units(stream, w_gu):
    partial = dot_nt(stream, w_gu).astype(BF16)
    cols = partial.shape[1] // 2
    summed = exchange(partial.reshape(4, -1, 2 * cols), "z").astype(F32).sum(axis=0)
    hidden = (jax.nn.silu(summed[:, :cols]) * summed[:, cols:]).astype(BF16)
    return share(hidden, "z", 4).reshape(-1, cols)


def per_device(inputs, gate_weight, up_weight, down_weight, norm_gain, norm_shift):
    c = lax.axis_index("c")
    x = lax.axis_index("x")
    y = lax.axis_index("y")
    half = inputs.shape[0] // 2
    quarter = half // 4
    mine = lax.dynamic_slice_in_dim(inputs, c * half + y * quarter, quarter, 0)
    rows = share(mine, "x", 4).transpose(1, 0, 2).reshape(quarter, 1024)
    stream = share(rows, "y", 4).reshape(half, 1024)
    affine = jnp.stack((norm_gain[0], norm_shift[0]))
    affine = lax.all_gather(affine, "x", axis=1, tiled=True)
    gu0, down0 = regroup_weights(gate_weight[0], up_weight[0], down_weight[0])
    gu1, down1 = regroup_weights(gate_weight[1], up_weight[1], down_weight[1])
    hidden = hidden_units(stream, gu0)
    partial = jnp.dot(hidden, down0, preferred_element_type=F32).astype(BF16)
    block = half // 16
    branch = exchange(partial.reshape(16, block, 1024), ("x", "y")).astype(F32).sum(axis=0)
    own = lax.dynamic_slice_in_dim(stream, (x * 4 + y) * block, block, 0)
    mixed = RESIDUAL * own.astype(F32) + branch
    stats = lax.psum(jnp.stack((mixed.sum(axis=1), (mixed * mixed).sum(axis=1))), "z")
    out = normed(mixed, stats[0], stats[1], affine[0], affine[1])
    stream = share(out, ("x", "y"), 16).reshape(half, 1024)
    hidden = hidden_units(stream, gu1)
    partial = jnp.dot(hidden, down1, preferred_element_type=F32).astype(BF16)
    parts = partial.reshape(4, quarter, 4, 256).transpose(2, 0, 1, 3).reshape(16, quarter, 256)
    branch = exchange(parts, ("x", "y")).astype(F32).sum(axis=0)
    own = lax.dynamic_slice(stream, (y * quarter, x * 256), (quarter, 256))
    mixed = RESIDUAL * own.astype(F32) + branch
    stats = lax.psum(jnp.stack((mixed.sum(axis=1), (mixed * mixed).sum(axis=1))), ("z", "x"))
    out = normed(mixed, stats[0], stats[1], norm_gain[1], norm_shift[1])
    ours = share(out, "y", 4).reshape(half, 256)
    theirs = swap_core(ours)
    result = jnp.concatenate((ours, theirs), axis=0)
    swapped = jnp.concatenate((theirs, ours), axis=0)
    return jnp.where(c == 0, result, swapped)


def solution(mesh):
    finer = Mesh(mesh.devices.reshape(4, 4, 4, 2), ("z", "x", "y", "c"))
    ra, cb = (("z", "x"), ("y", "c"))
    in_specs = (
        P(None, ra),
        P(None, ra, cb),
        P(None, ra, cb),
        P(None, cb, ra),
        P(None, ra),
        P(None, ra),
    )
    return jax.shard_map(
        per_device, mesh=finer, in_specs=in_specs, out_specs=P(None, ra), check_vma=False
    )
```

profile of v0, /device:TPU:1, one launch (start us, length us, event | category | flops | bytes accessed | tf_op | source)
XLA Modules:
  0.0 365.9 jit_solution(2115882943331297913)
XLA Ops:
  0.0 2.4 fusion.6
  2.7 2.3 fusion.7
  5.2 2.3 fusion.8
  7.9 30.5 %all_to_all.60 = bf16[4,3,352,256]{3,2,1,0:T(8,128)(2,1)S(1)} all-to-all(bf16[4,3,352,256]{3,2,1,0:T(8,128)(2,1)S(1)} %copy.30), channel_id=1, replica_groups=mesh['z'=4,'x'=4,'y'=4,'c'=2] {'x'}, dimensions={0} | all-to-all | bytes 4325376 | tf_op jit(solution)/shard_map/all_to_all | solution.py:14
  38.7 2.2 collective-permute-start
  41.0 10.2 %all_to_all.61 = bf16[4,192,256]{2,1,0:T(8,128)(2,1)S(1)} all-to-all(bf16[4,192,256]{2,1,0:T(8,128)(2,1)S(1)} %broadcast_in_dim.14), channel_id=1, replica_groups=mesh['z'=4,'x'=4,'y'=4,'c'=2] {'x'}, dimensions={0} | all-to-all | bytes 786432 | tf_op jit(solution)/shard_map/all_to_all | solution.py:14
  51.2 1.4 broadcast_in_dim.16
  52.7 4.4 %all-to-all-start.1 = ((bf16[4,192,1024]{2,1,0:T(8,128)(2,1)}), bf16[4,192,1024]{2,1,0:T(8,128)(2,1)}, u32[]{:S(2)}, u32[]{:S(2)}) async-start(bf16[4,192,1024]{2,1,0:T(8,128)(2,1)} %broadcast_in_dim.16), calls=%async_computation.1 | async-start | bytes 3145728 | tf_op jit(solution)/shard_map/all_to_all | solution.py:14
  57.2 1.8 constant_dynamic-update-slice_fusion
  59.0 2.0 copy-done.2
  61.1 1.9 slice.96
  62.9 13.6 %all-to-all-done.1 = bf16[4,192,1024]{2,1,0:T(8,128)(2,1)} async-done(((bf16[4,192,1024]{2,1,0:T(8,128)(2,1)}), bf16[4,192,1024]{2,1,0:T(8,128)(2,1)}, u32[]{:S(2)}, u32[]{:S(2)}) %all-to-all-start.1) | async-done | bytes 1572896 | tf_op jit(solution)/shard_map/all_to_all | solution.py:14
  76.5 4.9 %convolution_convert_fusion.1 = bf16[768,1408]{1,0:T(8,128)(2,1)S(1)} fusion(bf16[768,1024]{1,0:T(8,128)(2,1)} %bitcast.1, bf16[1408,1024]{1,0:T(8,128)(2,1)} %bitcast.85), kind=kOutput, calls=%fused_computation.3 | convolution fusion | flops 2215673856 | bytes 6619136 | tf_op jit(solution)/shard_map/dot_general | solution.py:26
  81.5 29.2 %all_to_all.62 = bf16[4,192,1408]{2,1,0:T(8,128)(2,1)S(1)} all-to-all(bf16[4,192,1408]{2,1,0:T(8,128)(2,1)S(1)} %bitcast.93), channel_id=1, replica_groups=mesh['z'=4,'x'=4,'y'=4,'c'=2] {'z'}, dimensions={0} | all-to-all | bytes 4325376 | tf_op jit(solution)/shard_map/all_to_all | solution.py:14
  111.2 1.2 broadcast_in_dim.17
  112.4 4.4 %all-to-all-start.4 = ((bf16[4,192,704]{2,1,0:T(8,128)(2,1)}), bf16[4,192,704]{2,1,0:T(8,128)(2,1)}, u32[]{:S(2)}, u32[]{:S(2)}) async-start(bf16[4,192,704]{2,1,0:T(8,128)(2,1)} %broadcast_in_dim.17), calls=%async_computation.4 | async-start | bytes 2359296 | tf_op jit(solution)/shard_map/all_to_all | solution.py:14
  117.6 1.5 copy.34
  119.1 10.4 %all-to-all-done.4 = bf16[4,192,704]{2,1,0:T(8,128)(2,1)} async-done(((bf16[4,192,704]{2,1,0:T(8,128)(2,1)}), bf16[4,192,704]{2,1,0:T(8,128)(2,1)}, u32[]{:S(2)}, u32[]{:S(2)}) %all-to-all-start.4) | async-done | bytes 1081376 | tf_op jit(solution)/shard_map/all_to_all | solution.py:14
  129.5 3.6 all-to-all-start.7
  133.2 4.3 %convolution_convert_fusion.3 = bf16[768,1024]{1,0:T(8,128)(2,1)} fusion(bf16[768,704]{1,0:T(8,128)(2,1)} %bitcast.13, bf16[3,704,1024]{2,1,0:T(8,128)(2,1)} %copy-done.2), kind=kOutput, calls=%fused_computation.9 | convolution fusion | flops 1108082688 | bytes 4194304 | tf_op jit(solution)/shard_map/dot_general | solution.py:69
  137.5 18.0 %all-to-all-done.7 = bf16[4,3,352,256]{3,2,1,0:T(8,128)(2,1)S(1)} async-done(((bf16[4,3,352,256]{3,2,1,0:T(8,128)(2,1)}), bf16[4,3,352,256]{3,2,1,0:T(8,128)(2,1)S(1)}, u32[]{:S(2)}, u32[]{:S(2)}) %all-to-all-start.7) | async-done | bytes 2162720 | tf_op jit(solution)/shard_map/all_to_all | solution.py:14
  155.5 4.4 %all-to-all-start.5 = ((bf16[16,48,1024]{2,1,0:T(8,128)(2,1)}), bf16[16,48,1024]{2,1,0:T(8,128)(2,1)}, u32[]{:S(2)}, u32[]{:S(2)}) async-start(bf16[16,48,1024]{2,1,0:T(8,128)(2,1)} %bitcast.95), calls=%async_computation.5 | async-start | bytes 3145728 | tf_op jit(solution)/shard_map/all_to_all | solution.py:14
  160.0 18.8 %all_gather.3 = f32[2,1024]{1,0:T(2,128)S(1)} all-gather(f32[2,256]{1,0:T(2,128)S(1)} %pad_maximum_fusion), channel_id=1, replica_groups=mesh['z'=4,'x'=4,'y'=4,'c'=2] {'x'}, dimensions={1}, use_global_device_ids=true | all-gather | bytes 10240 | tf_op jit(solution)/shard_map/all_gather | solution.py:65
  178.8 1.6 copy.43
  180.4 8.3 %collective-permute-start.1 = (bf16[3,352,1024]{2,1,0:T(8,128)(2,1)}, bf16[3,352,1024]{2,1,0:T(8,128)(2,1)S(1)}, u32[]{:S(2)}, u32[]{:S(2)}) collective-permute-start(bf16[3,352,1024]{2,1,0:T(8,128)(2,1)} %bitcast.59), channel_id=1, source_target_pairs={{0,1},{1,0},{2,3},{3,2},{4,5},{5,4},{6,7},{7,6},{8,9},{9,8},{10,11... | collective-permute-start | bytes 6488072 | tf_op jit(solution)/shard_map/ppermute | solution.py:22
  188.8 1.7 convert_reduce_fusion.3
  190.5 1.0 fusion.2
  191.5 6.9 %psum.14 = f32[2,48]{1,0:T(2,128)S(1)} all-reduce(f32[2,48]{1,0:T(2,128)S(1)} %pad_maximum_fusion.2), channel_id=1, replica_groups=mesh['z'=4,'x'=4,'y'=4,'c'=2] {'z'}, use_global_device_ids=true, to_apply=%region_4.5 | all-reduce | flops 96 | bytes 768 | tf_op jit(solution)/shard_map/psum | solution.py:74
  199.4 1.4 broadcast_in_dim.18
  200.8 5.1 %all-to-all-start.6 = ((bf16[16,48,1024]{2,1,0:T(8,128)(2,1)}), bf16[16,48,1024]{2,1,0:T(8,128)(2,1)}, u32[]{:S(2)}, u32[]{:S(2)}) async-start(bf16[16,48,1024]{2,1,0:T(8,128)(2,1)} %broadcast_in_dim.18), calls=%async_computation.6 | async-start | bytes 3145728 | tf_op jit(solution)/shard_map/all_to_all | solution.py:14
  205.9 1.8 constant_dynamic-update-slice_fusion.3
  207.9 2.0 copy-done.3
  209.9 1.9 slice.102
  211.8 14.5 %all-to-all-done.6 = bf16[16,48,1024]{2,1,0:T(8,128)(2,1)} async-done(((bf16[16,48,1024]{2,1,0:T(8,128)(2,1)}), bf16[16,48,1024]{2,1,0:T(8,128)(2,1)}, u32[]{:S(2)}, u32[]{:S(2)}) %all-to-all-start.6) | async-done | bytes 1572896 | tf_op jit(solution)/shard_map/all_to_all | solution.py:14
  226.3 4.9 %convolution_convert_fusion = bf16[768,1408]{1,0:T(8,128)(2,1)S(1)} fusion(bf16[768,1024]{1,0:T(8,128)(2,1)} %bitcast.22, bf16[1408,1024]{1,0:T(8,128)(2,1)} %bitcast.86), kind=kOutput, calls=%fused_computation.2 | convolution fusion | flops 2215673856 | bytes 6619136 | tf_op jit(solution)/shard_map/dot_general | solution.py:26
  231.3 25.4 %all_to_all.63 = bf16[4,192,1408]{2,1,0:T(8,128)(2,1)S(1)} all-to-all(bf16[4,192,1408]{2,1,0:T(8,128)(2,1)S(1)} %bitcast.94), channel_id=1, replica_groups=mesh['z'=4,'x'=4,'y'=4,'c'=2] {'z'}, dimensions={0} | all-to-all | bytes 4325376 | tf_op jit(solution)/shard_map/all_to_all | solution.py:14
  257.4 13.7 %all_to_all.64 = bf16[4,192,704]{2,1,0:T(8,128)(2,1)S(1)} all-to-all(bf16[4,192,704]{2,1,0:T(8,128)(2,1)S(1)} %broadcast_in_dim.19), channel_id=1, replica_groups=mesh['z'=4,'x'=4,'y'=4,'c'=2] {'z'}, dimensions={0} | all-to-all | bytes 2162688 | tf_op jit(solution)/shard_map/all_to_all | solution.py:14
  271.1 3.9 %convolution_convert_fusion.2 = bf16[768,1024]{1,0:T(8,128)(2,1)} fusion(bf16[768,704]{1,0:T(8,128)(2,1)S(1)} %bitcast.100, bf16[3,704,1024]{2,1,0:T(8,128)(2,1)} %copy-done.3), kind=kOutput, calls=%fused_computation.8 | convolution fusion | flops 1108082688 | bytes 4096000 | tf_op jit(solution)/shard_map/dot_general | solution.py:78
  275.0 2.9 reshape.113
  277.9 1.4 copy.36
  279.3 10.2 %all-to-all-start.10 = ((bf16[16,192,256]{2,1,0:T(8,128)(2,1)}), bf16[16,192,256]{2,1,0:T(8,128)(2,1)S(1)}, u32[]{:S(2)}, u32[]{:S(2)}) async-start(bf16[16,192,256]{2,1,0:T(8,128)(2,1)} %bitcast.84), calls=%async_computation.10 | async-start | bytes 3145728 | tf_op jit(solution)/shard_map/all_to_all | solution.py:14
  289.6 19.0 %all-to-all-done.10 = bf16[16,192,256]{2,1,0:T(8,128)(2,1)S(1)} async-done(((bf16[16,192,256]{2,1,0:T(8,128)(2,1)}), bf16[16,192,256]{2,1,0:T(8,128)(2,1)S(1)}, u32[]{:S(2)}, u32[]{:S(2)}) %all-to-all-start.10) | async-done | bytes 1572896 | tf_op jit(solution)/shard_map/all_to_all | solution.py:14
  308.8 1.1 fusion.3
  309.9 31.9 %psum.15 = f32[2,192]{1,0:T(2,128)S(1)} all-reduce(f32[2,192]{1,0:T(2,128)S(1)} %pad_maximum_fusion.1), channel_id=1, replica_groups=mesh['z'=4,'x'=4,'y'=4,'c'=2] {'z','x'}, use_global_device_ids=true, to_apply=%region_9.10 | all-reduce | flops 384 | bytes 3072 | tf_op jit(solution)/shard_map/psum | solution.py:83
  342.9 10.1 %all_to_all.65 = bf16[4,192,256]{2,1,0:T(8,128)(2,1)S(1)} all-to-all(bf16[4,192,256]{2,1,0:T(8,128)(2,1)S(1)} %broadcast_in_dim.20), channel_id=1, replica_groups=mesh['z'=4,'x'=4,'y'=4,'c'=2] {'y'}, dimensions={0} | all-to-all | bytes 786432 | tf_op jit(solution)/shard_map/all_to_all | solution.py:14
  353.0 10.3 %collective-permute-start.2 = (bf16[768,256]{1,0:T(8,128)(2,1)S(1)}, bf16[768,256]{1,0:T(8,128)(2,1)S(1)}, u32[]{:S(2)}, u32[]{:S(2)}) collective-permute-start(bf16[768,256]{1,0:T(8,128)(2,1)S(1)} %bitcast.97), channel_id=1, source_target_pairs={{0,1},{1,0},{2,3},{3,2},{4,5},{5,4},{6,7},{7,6},{8,9},{9,8},{10,11... | collective-permute-start | bytes 1179656 | tf_op jit(solution)/shard_map/ppermute | solution.py:22
  363.3 1.3 collective-permute-done.2
  364.7 1.2 maximum_select_fusion
  (50 shorter events, 6.0 us)
Async XLA Ops:
  0.0 40.9 %copy-start = (bf16[1536,256]{1,0:T(8,128)(2,1)S(1)}, bf16[1536,256]{1,0:T(8,128)(2,1)}, u32[]{:S(2)}) copy-start(bf16[1536,256]{1,0:T(8,128)(2,1)} %param.6) | copy-start | bytes 2359300
  38.7 18.5 %collective-permute-start = (bf16[3,352,1024]{2,1,0:T(8,128)(2,1)S(1)}, bf16[3,352,1024]{2,1,0:T(8,128)(2,1)}, u32[]{:S(2)}, u32[]{:S(2)}) collective-permute-start(bf16[3,352,1024]{2,1,0:T(8,128)(2,1)S(1)} %bitcast.81), channel_id=1, source_target_pairs={{0,1},{1,0},{2,3},{3,2},{4,5},{5,4},{6,7},{7,6},{8,9},{9,8},{10,11... | collective-permute-start | bytes 6488072 | tf_op jit(solution)/shard_map/ppermute | solution.py:22
  52.7 23.9 %all-to-all-start.1 = ((bf16[4,192,1024]{2,1,0:T(8,128)(2,1)}), bf16[4,192,1024]{2,1,0:T(8,128)(2,1)}, u32[]{:S(2)}, u32[]{:S(2)}) async-start(bf16[4,192,1024]{2,1,0:T(8,128)(2,1)} %broadcast_in_dim.16), calls=%async_computation.1 | async-start | bytes 3145728 | tf_op jit(solution)/shard_map/all_to_all | solution.py:14
  59.0 2.1 copy-start.2
  111.2 5.6 %copy-start.4 = (bf16[1,256,1408]{2,1,0:T(8,128)(2,1)S(1)}, bf16[1,256,1408]{2,1,0:T(8,128)(2,1)}, u32[]{:S(2)}) copy-start(bf16[1,256,1408]{2,1,0:T(8,128)(2,1)} %get-tuple-element.9) | copy-start | bytes 2162692
  112.4 4.7 %copy-start.5 = (bf16[1,256,1408]{2,1,0:T(8,128)(2,1)S(1)}, bf16[1,256,1408]{2,1,0:T(8,128)(2,1)}, u32[]{:S(2)}) copy-start(bf16[1,256,1408]{2,1,0:T(8,128)(2,1)} %get-tuple-element.11) | copy-start | bytes 2162692
  112.4 5.0 %copy-start.6 = (bf16[1,1408,256]{2,1,0:T(8,128)(2,1)S(1)}, bf16[1,1408,256]{2,1,0:T(8,128)(2,1)}, u32[]{:S(2)}) copy-start(bf16[1,1408,256]{2,1,0:T(8,128)(2,1)} %get-tuple-element.13) | copy-start | bytes 2162692
  112.4 17.1 %all-to-all-start.4 = ((bf16[4,192,704]{2,1,0:T(8,128)(2,1)}), bf16[4,192,704]{2,1,0:T(8,128)(2,1)}, u32[]{:S(2)}, u32[]{:S(2)}) async-start(bf16[4,192,704]{2,1,0:T(8,128)(2,1)} %broadcast_in_dim.17), calls=%async_computation.4 | async-start | bytes 2359296 | tf_op jit(solution)/shard_map/all_to_all | solution.py:14
  129.5 25.9 %all-to-all-start.7 = ((bf16[4,3,352,256]{3,2,1,0:T(8,128)(2,1)}), bf16[4,3,352,256]{3,2,1,0:T(8,128)(2,1)S(1)}, u32[]{:S(2)}, u32[]{:S(2)}) async-start(bf16[4,3,352,256]{3,2,1,0:T(8,128)(2,1)} %copy.34), calls=%async_computation.7 | async-start | bytes 4325376 | tf_op jit(solution)/shard_map/all_to_all | solution.py:14
  137.5 22.4 %copy-start.7 = (f32[2,256]{1,0:T(2,128)S(1)}, f32[2,256]{1,0:T(2,128)}, u32[]{:S(2)}) copy-start(f32[2,256]{1,0:T(2,128)} %param.10) | copy-start | bytes 6148
  137.5 22.5 %copy-start.8 = (f32[2,256]{1,0:T(2,128)S(1)}, f32[2,256]{1,0:T(2,128)}, u32[]{:S(2)}) copy-start(f32[2,256]{1,0:T(2,128)} %param.11) | copy-start | bytes 6148
  155.5 33.3 %all-to-all-start.5 = ((bf16[16,48,1024]{2,1,0:T(8,128)(2,1)}), bf16[16,48,1024]{2,1,0:T(8,128)(2,1)}, u32[]{:S(2)}, u32[]{:S(2)}) async-start(bf16[16,48,1024]{2,1,0:T(8,128)(2,1)} %bitcast.95), calls=%async_computation.5 | async-start | bytes 3145728 | tf_op jit(solution)/shard_map/all_to_all | solution.py:14
  180.4 27.2 %collective-permute-start.1 = (bf16[3,352,1024]{2,1,0:T(8,128)(2,1)}, bf16[3,352,1024]{2,1,0:T(8,128)(2,1)S(1)}, u32[]{:S(2)}, u32[]{:S(2)}) collective-permute-start(bf16[3,352,1024]{2,1,0:T(8,128)(2,1)} %bitcast.59), channel_id=1, source_target_pairs={{0,1},{1,0},{2,3},{3,2},{4,5},{5,4},{6,7},{7,6},{8,9},{9,8},{10,11... | collective-permute-start | bytes 6488072 | tf_op jit(solution)/shard_map/ppermute | solution.py:22
  200.8 25.5 %all-to-all-start.6 = ((bf16[16,48,1024]{2,1,0:T(8,128)(2,1)}), bf16[16,48,1024]{2,1,0:T(8,128)(2,1)}, u32[]{:S(2)}, u32[]{:S(2)}) async-start(bf16[16,48,1024]{2,1,0:T(8,128)(2,1)} %broadcast_in_dim.18), calls=%async_computation.6 | async-start | bytes 3145728 | tf_op jit(solution)/shard_map/all_to_all | solution.py:14
  207.9 2.0 copy-start.3
  279.3 29.2 %all-to-all-start.10 = ((bf16[16,192,256]{2,1,0:T(8,128)(2,1)}), bf16[16,192,256]{2,1,0:T(8,128)(2,1)S(1)}, u32[]{:S(2)}, u32[]{:S(2)}) async-start(bf16[16,192,256]{2,1,0:T(8,128)(2,1)} %bitcast.84), calls=%async_computation.10 | async-start | bytes 3145728 | tf_op jit(solution)/shard_map/all_to_all | solution.py:14
  308.6 57.3 %copy-start.1 = (bf16[1536,256]{1,0:T(8,128)(2,1)S(1)}, bf16[1536,256]{1,0:T(8,128)(2,1)}, u32[]{:S(2)}) copy-start(bf16[1536,256]{1,0:T(8,128)(2,1)} %param.6) | copy-start | bytes 2359300
  353.0 11.7 %collective-permute-start.2 = (bf16[768,256]{1,0:T(8,128)(2,1)S(1)}, bf16[768,256]{1,0:T(8,128)(2,1)S(1)}, u32[]{:S(2)}, u32[]{:S(2)}) collective-permute-start(bf16[768,256]{1,0:T(8,128)(2,1)S(1)} %bitcast.97), channel_id=1, source_target_pairs={{0,1},{1,0},{2,3},{3,2},{4,5},{5,4},{6,7},{7,6},{8,9},{9,8},{10,11... | collective-permute-start | bytes 1179656 | tf_op jit(solution)/shard_map/ppermute | solution.py:22
where the time goes:
time: 367 us; the launch traced here: 366 us
  blocking collectives  177 us (48%)
  waiting for transfers between devices  76.9 us (21%)
  starting transfers between devices  52.9 us (14%)
  local copies, waits for them, and re-layouts  31.9 us (9%)
  matrix products  18.1 us (5%)
  other arithmetic  8.87 us (2%)
    all_to_all x6, blocking collectives, exchange(): return lax.all_to_all(parts, axes, 0, 0, tiled=True)  119 us
    all_to_all x6, waiting for transfers between devices, exchange(): return lax.all_to_all(parts, axes, 0, 0, tiled=True)  75.6 us
    all_to_all x6, starting transfers between devices, exchange(): return lax.all_to_all(parts, axes, 0, 0, tiled=True)  32.1 us
    psum x1, blocking collectives, per_device(): lax.psum(jnp.stack((mixed.sum(axis=1), (mixed * mixed).sum(axis=1))), ('z...  31.9 us
    ppermute x3, starting transfers between devices, swap_core(): return lax.ppermute(block, 'c', [(0, 1), (1, 0)])  20.8 us
    all_gather x1, blocking collectives, per_device(): affine = lax.all_gather(affine, 'x', axis=1, tiled=True)  18.8 us
    dot_general x2, matrix products, dot_nt(): lax.dot_general(a, b, (((1,), (1,)), ((), ())), preferred_element_type=F32)  9.85 us
  transfers between devices with their start and end apart: 9, of which 6 were waited for; matrix products, arithmetic and copies ran while one was open for 6% of the time, Pallas kernels for 0%

commit v1 on v0

--- a/solution.py
+++ b/solution.py
@@ -62,7 +62,9 @@
     rows = share(mine, "x", 4).transpose(1, 0, 2).reshape(quarter, 1024)
     stream = share(rows, "y", 4).reshape(half, 1024)
     affine = jnp.stack((norm_gain[0], norm_shift[0]))
-    affine = lax.all_gather(affine, "x", axis=1, tiled=True)
+    affine = jnp.concatenate(
+        lax.all_to_all(jnp.stack([affine] * lax.axis_size("x")), "x", 0, 0), axis=1
+    )
     gu0, down0 = regroup_weights(gate_weight[0], up_weight[0], down_weight[0])
     gu1, down1 = regroup_weights(gate_weight[1], up_weight[1], down_weight[1])
     hidden = hidden_units(stream, gu0)

time: 367 us -> 350 us (0.954)
  blocking collectives: 177 us -> 124 us
  waiting for transfers between devices: 76.9 us -> 101 us
  starting transfers between devices: 52.9 us -> 63.1 us
    all_to_all x6 -> x5, blocking collectives: 119 us -> 85.1 us  [exchange(): return lax.all_to_all(parts, axes, 0, 0, tiled=True)]
    all_to_all x6 -> x7, waiting for transfers between devices: 75.6 us -> 95.9 us  [exchange(): return lax.all_to_all(parts, axes, 0, 0, tiled=True)]
    all_gather x1 -> x0, blocking collectives: 18.8 us -> none  [per_device(): affine = lax.all_gather(affine, 'x', axis=1, tiled=True)]
    ppermute x3, starting transfers between devices: 20.8 us -> 28.9 us  [swap_core(): return lax.ppermute(block, 'c', [(0, 1), (1, 0)])]
    all_to_all x6 -> x7, starting transfers between devices: 32.1 us -> 31 us  [exchange(): return lax.all_to_all(parts, axes, 0, 0, tiled=True)]
  transfers between devices with their start and end apart: 9 -> 11, of which waited for: 6 -> 9; matrix products, arithmetic and copies ran while one was open for 6% -> 7% of each run, Pallas kernels for 0% -> 0%
where the time goes in v1:
time: 350 us; the launch traced here: 349 us
  blocking collectives  124 us (35%)
  waiting for transfers between devices  101 us (29%)
  starting transfers between devices  63.1 us (18%)
  local copies, waits for them, and re-layouts  32.4 us (9%)
  matrix products  19.5 us (6%)
  other arithmetic  8.85 us (3%)
    all_to_all x7, waiting for transfers between devices, exchange(): return lax.all_to_all(parts, axes, 0, 0, tiled=True)  95.9 us
    all_to_all x5, blocking collectives, exchange(): return lax.all_to_all(parts, axes, 0, 0, tiled=True)  85.1 us
    psum x1, blocking collectives, per_device(): lax.psum(jnp.stack((mixed.sum(axis=1), (mixed * mixed).sum(axis=1))), ('z...  32 us
    all_to_all x7, starting transfers between devices, exchange(): return lax.all_to_all(parts, axes, 0, 0, tiled=True)  31 us
    ppermute x3, starting transfers between devices, swap_core(): return lax.ppermute(block, 'c', [(0, 1), (1, 0)])  28.9 us
    dot_general x2, matrix products, dot_nt(): lax.dot_general(a, b, (((1,), (1,)), ((), ())), preferred_element_type=F32)  11.3 us
    unnamed x24, local copies, waits for them, and re-layouts  7.07 us
    psum x1, blocking collectives, per_device(): lax.psum(jnp.stack((mixed.sum(axis=1), (mixed * mixed).sum(axis=1))), 'z')  7.02 us
  transfers between devices with their start and end apart: 11, of which 9 were waited for; matrix products, arithmetic and copies ran while one was open for 7% of the time, Pallas kernels for 0%

profile of v1, /device:TPU:1, one launch (start us, length us, event | category | flops | bytes accessed | tf_op | source)
XLA Modules:
  0.0 349.0 jit_solution(13439448667863027433)
XLA Ops:
  0.0 2.4 fusion.6
  2.6 2.3 fusion.7
  5.3 2.3 fusion.8
  7.9 30.5 %all_to_all.65 = bf16[4,3,352,256]{3,2,1,0:T(8,128)(2,1)S(1)} all-to-all(bf16[4,3,352,256]{3,2,1,0:T(8,128)(2,1)S(1)} %copy.30), channel_id=1, replica_groups=mesh['z'=4,'x'=4,'y'=4,'c'=2] {'x'}, dimensions={0} | all-to-all | bytes 4325376 | tf_op jit(solution)/shard_map/all_to_all | solution.py:14
  38.7 2.2 collective-permute-start
  41.0 10.2 %all_to_all.66 = bf16[4,192,256]{2,1,0:T(8,128)(2,1)S(1)} all-to-all(bf16[4,192,256]{2,1,0:T(8,128)(2,1)S(1)} %broadcast_in_dim.14), channel_id=1, replica_groups=mesh['z'=4,'x'=4,'y'=4,'c'=2] {'x'}, dimensions={0} | all-to-all | bytes 786432 | tf_op jit(solution)/shard_map/all_to_all | solution.py:14
  51.2 1.4 broadcast_in_dim.16
  52.7 4.3 %all-to-all-start.1 = ((bf16[4,192,1024]{2,1,0:T(8,128)(2,1)}), bf16[4,192,1024]{2,1,0:T(8,128)(2,1)}, u32[]{:S(2)}, u32[]{:S(2)}) async-start(bf16[4,192,1024]{2,1,0:T(8,128)(2,1)} %broadcast_in_dim.16), calls=%async_computation.1 | async-start | bytes 3145728 | tf_op jit(solution)/shard_map/all_to_all | solution.py:14
  57.2 1.8 constant_dynamic-update-slice_fusion
  59.0 2.0 copy-done.2
  61.0 1.9 slice.98
  62.9 13.7 %all-to-all-done.1 = bf16[4,192,1024]{2,1,0:T(8,128)(2,1)} async-done(((bf16[4,192,1024]{2,1,0:T(8,128)(2,1)}), bf16[4,192,1024]{2,1,0:T(8,128)(2,1)}, u32[]{:S(2)}, u32[]{:S(2)}) %all-to-all-start.1) | async-done | bytes 1572896 | tf_op jit(solution)/shard_map/all_to_all | solution.py:14
  76.5 6.3 %convolution_convert_fusion.1 = bf16[768,1408]{1,0:T(8,128)(2,1)} fusion(bf16[768,1024]{1,0:T(8,128)(2,1)} %bitcast.1, bf16[1408,1024]{1,0:T(8,128)(2,1)} %bitcast.86), kind=kOutput, calls=%fused_computation.3 | convolution fusion | flops 2215673856 | bytes 6619136 | tf_op jit(solution)/shard_map/dot_general | solution.py:26
  82.9 5.2 %all-to-all-start.3 = ((bf16[4,192,1408]{2,1,0:T(8,128)(2,1)}), bf16[4,192,1408]{2,1,0:T(8,128)(2,1)S(1)}, u32[]{:S(2)}, u32[]{:S(2)}) async-start(bf16[4,192,1408]{2,1,0:T(8,128)(2,1)} %bitcast.94), calls=%async_computation.3 | async-start | bytes 4325376 | tf_op jit(solution)/shard_map/all_to_all | solution.py:14
  88.1 24.6 %all-to-all-done.3 = bf16[4,192,1408]{2,1,0:T(8,128)(2,1)S(1)} async-done(((bf16[4,192,1408]{2,1,0:T(8,128)(2,1)}), bf16[4,192,1408]{2,1,0:T(8,128)(2,1)S(1)}, u32[]{:S(2)}, u32[]{:S(2)}) %all-to-all-start.3) | async-done | bytes 2162720 | tf_op jit(solution)/shard_map/all_to_all | solution.py:14
  113.3 3.2 all-to-all-start.6
  117.0 3.6 %all-to-all-done.6 = f32[4,2,256]{2,1,0:T(2,128)S(1)} async-done(((f32[4,2,256]{2,1,0:T(2,128)}), f32[4,2,256]{2,1,0:T(2,128)S(1)}, u32[]{:S(2)}, u32[]{:S(2)}) %all-to-all-start.6) | async-done | bytes 8224 | tf_op jit(solution)/shard_map/all_to_all | solution.py:66
  121.7 4.4 %all-to-all-start.4 = ((bf16[4,192,704]{2,1,0:T(8,128)(2,1)}), bf16[4,192,704]{2,1,0:T(8,128)(2,1)}, u32[]{:S(2)}, u32[]{:S(2)}) async-start(bf16[4,192,704]{2,1,0:T(8,128)(2,1)} %broadcast_in_dim.17), calls=%async_computation.4 | async-start | bytes 2359296 | tf_op jit(solution)/shard_map/all_to_all | solution.py:14
  127.0 1.5 copy.34
  128.5 9.5 %all-to-all-done.4 = bf16[4,192,704]{2,1,0:T(8,128)(2,1)} async-done(((bf16[4,192,704]{2,1,0:T(8,128)(2,1)}), bf16[4,192,704]{2,1,0:T(8,128)(2,1)}, u32[]{:S(2)}, u32[]{:S(2)}) %all-to-all-start.4) | async-done | bytes 1081376 | tf_op jit(solution)/shard_map/all_to_all | solution.py:14
  138.0 3.6 %all-to-all-start.8 = ((bf16[4,3,352,256]{3,2,1,0:T(8,128)(2,1)}), bf16[4,3,352,256]{3,2,1,0:T(8,128)(2,1)S(1)}, u32[]{:S(2)}, u32[]{:S(2)}) async-start(bf16[4,3,352,256]{3,2,1,0:T(8,128)(2,1)} %copy.34), calls=%async_computation.8 | async-start | bytes 4325376 | tf_op jit(solution)/shard_map/all_to_all | solution.py:14
  141.7 4.3 %convolution_convert_fusion.3 = bf16[768,1024]{1,0:T(8,128)(2,1)} fusion(bf16[768,704]{1,0:T(8,128)(2,1)} %bitcast.13, bf16[3,704,1024]{2,1,0:T(8,128)(2,1)} %copy-done.2), kind=kOutput, calls=%fused_computation.9 | convolution fusion | flops 1108082688 | bytes 4194304 | tf_op jit(solution)/shard_map/dot_general | solution.py:71
  145.9 16.9 %all-to-all-done.8 = bf16[4,3,352,256]{3,2,1,0:T(8,128)(2,1)S(1)} async-done(((bf16[4,3,352,256]{3,2,1,0:T(8,128)(2,1)}), bf16[4,3,352,256]{3,2,1,0:T(8,128)(2,1)S(1)}, u32[]{:S(2)}, u32[]{:S(2)}) %all-to-all-start.8) | async-done | bytes 2162720 | tf_op jit(solution)/shard_map/all_to_all | solution.py:14
  162.8 4.4 %all-to-all-start.5 = ((bf16[16,48,1024]{2,1,0:T(8,128)(2,1)}), bf16[16,48,1024]{2,1,0:T(8,128)(2,1)}, u32[]{:S(2)}, u32[]{:S(2)}) async-start(bf16[16,48,1024]{2,1,0:T(8,128)(2,1)} %bitcast.96), calls=%async_computation.5 | async-start | bytes 3145728 | tf_op jit(solution)/shard_map/all_to_all | solution.py:14
  167.2 1.7 copy.43
  168.9 6.8 %collective-permute-start.1 = (bf16[3,352,1024]{2,1,0:T(8,128)(2,1)}, bf16[3,352,1024]{2,1,0:T(8,128)(2,1)S(1)}, u32[]{:S(2)}, u32[]{:S(2)}) collective-permute-start(bf16[3,352,1024]{2,1,0:T(8,128)(2,1)} %bitcast.60), channel_id=1, source_target_pairs={{0,1},{1,0},{2,3},{3,2},{4,5},{5,4},{6,7},{7,6},{8,9},{9,8},{10,11... | collective-permute-start | bytes 6488072 | tf_op jit(solution)/shard_map/ppermute | solution.py:22
  175.7 6.9 %all-to-all-done.5 = bf16[16,48,1024]{2,1,0:T(8,128)(2,1)} async-done(((bf16[16,48,1024]{2,1,0:T(8,128)(2,1)}), bf16[16,48,1024]{2,1,0:T(8,128)(2,1)}, u32[]{:S(2)}, u32[]{:S(2)}) %all-to-all-start.5) | async-done | bytes 1572896 | tf_op jit(solution)/shard_map/all_to_all | solution.py:14
  182.6 1.7 convert_reduce_fusion.3
  185.4 7.0 %psum.14 = f32[2,48]{1,0:T(2,128)S(1)} all-reduce(f32[2,48]{1,0:T(2,128)S(1)} %pad_maximum_fusion.2), channel_id=1, replica_groups=mesh['z'=4,'x'=4,'y'=4,'c'=2] {'z'}, use_global_device_ids=true, to_apply=%region_4.5 | all-reduce | flops 96 | bytes 768 | tf_op jit(solution)/shard_map/psum | solution.py:76
  193.4 1.4 broadcast_in_dim.18
  194.8 5.3 %all-to-all-start.7 = ((bf16[16,48,1024]{2,1,0:T(8,128)(2,1)}), bf16[16,48,1024]{2,1,0:T(8,128)(2,1)}, u32[]{:S(2)}, u32[]{:S(2)}) async-start(bf16[16,48,1024]{2,1,0:T(8,128)(2,1)} %broadcast_in_dim.18), calls=%async_computation.7 | async-start | bytes 3145728 | tf_op jit(solution)/shard_map/all_to_all | solution.py:14
  200.1 1.8 constant_dynamic-update-slice_fusion.3
  202.1 2.0 copy-done.3
  204.1 1.9 slice.104
  206.0 9.4 %all-to-all-done.7 = bf16[16,48,1024]{2,1,0:T(8,128)(2,1)} async-done(((bf16[16,48,1024]{2,1,0:T(8,128)(2,1)}), bf16[16,48,1024]{2,1,0:T(8,128)(2,1)}, u32[]{:S(2)}, u32[]{:S(2)}) %all-to-all-start.7) | async-done | bytes 1572896 | tf_op jit(solution)/shard_map/all_to_all | solution.py:14
  215.4 4.9 %convolution_convert_fusion = bf16[768,1408]{1,0:T(8,128)(2,1)S(1)} fusion(bf16[768,1024]{1,0:T(8,128)(2,1)} %bitcast.23, bf16[1408,1024]{1,0:T(8,128)(2,1)} %bitcast.87), kind=kOutput, calls=%fused_computation.2 | convolution fusion | flops 2215673856 | bytes 6619136 | tf_op jit(solution)/shard_map/dot_general | solution.py:26
  220.3 19.0 %all_to_all.67 = bf16[4,192,1408]{2,1,0:T(8,128)(2,1)S(1)} all-to-all(bf16[4,192,1408]{2,1,0:T(8,128)(2,1)S(1)} %bitcast.95), channel_id=1, replica_groups=mesh['z'=4,'x'=4,'y'=4,'c'=2] {'z'}, dimensions={0} | all-to-all | bytes 4325376 | tf_op jit(solution)/shard_map/all_to_all | solution.py:14
  240.0 16.4 %all_to_all.68 = bf16[4,192,704]{2,1,0:T(8,128)(2,1)S(1)} all-to-all(bf16[4,192,704]{2,1,0:T(8,128)(2,1)S(1)} %broadcast_in_dim.19), channel_id=1, replica_groups=mesh['z'=4,'x'=4,'y'=4,'c'=2] {'z'}, dimensions={0} | all-to-all | bytes 2162688 | tf_op jit(solution)/shard_map/all_to_all | solution.py:14
  256.4 3.9 %convolution_convert_fusion.2 = bf16[768,1024]{1,0:T(8,128)(2,1)} fusion(bf16[768,704]{1,0:T(8,128)(2,1)S(1)} %bitcast.101, bf16[3,704,1024]{2,1,0:T(8,128)(2,1)} %copy-done.3), kind=kOutput, calls=%fused_computation.8 | convolution fusion | flops 1108082688 | bytes 4096000 | tf_op jit(solution)/shard_map/dot_general | solution.py:80
  260.3 2.9 reshape.124
  263.2 1.4 copy.36
  264.6 3.7 %all-to-all-start.11 = ((bf16[16,192,256]{2,1,0:T(8,128)(2,1)}), bf16[16,192,256]{2,1,0:T(8,128)(2,1)S(1)}, u32[]{:S(2)}, u32[]{:S(2)}) async-start(bf16[16,192,256]{2,1,0:T(8,128)(2,1)} %bitcast.85), calls=%async_computation.11 | async-start | bytes 3145728 | tf_op jit(solution)/shard_map/all_to_all | solution.py:14
  268.4 14.9 %all-to-all-done.11 = bf16[16,192,256]{2,1,0:T(8,128)(2,1)S(1)} async-done(((bf16[16,192,256]{2,1,0:T(8,128)(2,1)}), bf16[16,192,256]{2,1,0:T(8,128)(2,1)S(1)}, u32[]{:S(2)}, u32[]{:S(2)}) %all-to-all-start.11) | async-done | bytes 1572896 | tf_op jit(solution)/shard_map/all_to_all | solution.py:14
  284.6 32.0 %psum.15 = f32[2,192]{1,0:T(2,128)S(1)} all-reduce(f32[2,192]{1,0:T(2,128)S(1)} %pad_maximum_fusion.1), channel_id=1, replica_groups=mesh['z'=4,'x'=4,'y'=4,'c'=2] {'z','x'}, use_global_device_ids=true, to_apply=%region_9.10 | all-reduce | flops 384 | bytes 3072 | tf_op jit(solution)/shard_map/psum | solution.py:85
  317.7 8.9 %all_to_all.69 = bf16[4,192,256]{2,1,0:T(8,128)(2,1)S(1)} all-to-all(bf16[4,192,256]{2,1,0:T(8,128)(2,1)S(1)} %broadcast_in_dim.20), channel_id=1, replica_groups=mesh['z'=4,'x'=4,'y'=4,'c'=2] {'y'}, dimensions={0} | all-to-all | bytes 786432 | tf_op jit(solution)/shard_map/all_to_all | solution.py:14
  326.6 19.9 %collective-permute-start.2 = (bf16[768,256]{1,0:T(8,128)(2,1)S(1)}, bf16[768,256]{1,0:T(8,128)(2,1)S(1)}, u32[]{:S(2)}, u32[]{:S(2)}) collective-permute-start(bf16[768,256]{1,0:T(8,128)(2,1)S(1)} %bitcast.98), channel_id=1, source_target_pairs={{0,1},{1,0},{2,3},{3,2},{4,5},{5,4},{6,7},{7,6},{8,9},{9,8},{10,11... | collective-permute-start | bytes 1179656 | tf_op jit(solution)/shard_map/ppermute | solution.py:22
  346.4 1.3 collective-permute-done.2
  347.8 1.2 maximum_select_fusion
  (53 shorter events, 9.8 us)
Async XLA Ops:
  0.0 40.9 %copy-start = (bf16[1536,256]{1,0:T(8,128)(2,1)S(1)}, bf16[1536,256]{1,0:T(8,128)(2,1)}, u32[]{:S(2)}) copy-start(bf16[1536,256]{1,0:T(8,128)(2,1)} %param.6) | copy-start | bytes 2359300
  38.7 18.5 %collective-permute-start = (bf16[3,352,1024]{2,1,0:T(8,128)(2,1)S(1)}, bf16[3,352,1024]{2,1,0:T(8,128)(2,1)}, u32[]{:S(2)}, u32[]{:S(2)}) collective-permute-start(bf16[3,352,1024]{2,1,0:T(8,128)(2,1)S(1)} %bitcast.81), channel_id=1, source_target_pairs={{0,1},{1,0},{2,3},{3,2},{4,5},{5,4},{6,7},{7,6},{8,9},{9,8},{10,11... | collective-permute-start | bytes 6488072 | tf_op jit(solution)/shard_map/ppermute | solution.py:22
  52.7 23.9 %all-to-all-start.1 = ((bf16[4,192,1024]{2,1,0:T(8,128)(2,1)}), bf16[4,192,1024]{2,1,0:T(8,128)(2,1)}, u32[]{:S(2)}, u32[]{:S(2)}) async-start(bf16[4,192,1024]{2,1,0:T(8,128)(2,1)} %broadcast_in_dim.16), calls=%async_computation.1 | async-start | bytes 3145728 | tf_op jit(solution)/shard_map/all_to_all | solution.py:14
  59.0 2.0 copy-start.2
  82.9 5.2 %copy-start.7 = (f32[2,256]{1,0:T(2,128)S(1)}, f32[2,256]{1,0:T(2,128)}, u32[]{:S(2)}) copy-start(f32[2,256]{1,0:T(2,128)} %param.10) | copy-start | bytes 6148
  82.9 5.2 %copy-start.8 = (f32[2,256]{1,0:T(2,128)S(1)}, f32[2,256]{1,0:T(2,128)}, u32[]{:S(2)}) copy-start(f32[2,256]{1,0:T(2,128)} %param.11) | copy-start | bytes 6148
  82.9 29.8 %all-to-all-start.3 = ((bf16[4,192,1408]{2,1,0:T(8,128)(2,1)}), bf16[4,192,1408]{2,1,0:T(8,128)(2,1)S(1)}, u32[]{:S(2)}, u32[]{:S(2)}) async-start(bf16[4,192,1408]{2,1,0:T(8,128)(2,1)} %bitcast.94), calls=%async_computation.3 | async-start | bytes 4325376 | tf_op jit(solution)/shard_map/all_to_all | solution.py:14
  113.3 7.4 %all-to-all-start.6 = ((f32[4,2,256]{2,1,0:T(2,128)}), f32[4,2,256]{2,1,0:T(2,128)S(1)}, u32[]{:S(2)}, u32[]{:S(2)}) async-start(f32[4,2,256]{2,1,0:T(2,128)} %stack.58), calls=%async_computation.6 | async-start | bytes 16384 | tf_op jit(solution)/shard_map/all_to_all | solution.py:66
  117.0 9.1 %copy-start.4 = (bf16[1,256,1408]{2,1,0:T(8,128)(2,1)S(1)}, bf16[1,256,1408]{2,1,0:T(8,128)(2,1)}, u32[]{:S(2)}) copy-start(bf16[1,256,1408]{2,1,0:T(8,128)(2,1)} %get-tuple-element.9) | copy-start | bytes 2162692
  121.7 4.7 %copy-start.5 = (bf16[1,256,1408]{2,1,0:T(8,128)(2,1)S(1)}, bf16[1,256,1408]{2,1,0:T(8,128)(2,1)}, u32[]{:S(2)}) copy-start(bf16[1,256,1408]{2,1,0:T(8,128)(2,1)} %get-tuple-element.11) | copy-start | bytes 2162692
  121.7 5.0 %copy-start.6 = (bf16[1,1408,256]{2,1,0:T(8,128)(2,1)S(1)}, bf16[1,1408,256]{2,1,0:T(8,128)(2,1)}, u32[]{:S(2)}) copy-start(bf16[1,1408,256]{2,1,0:T(8,128)(2,1)} %get-tuple-element.13) | copy-start | bytes 2162692
  121.7 16.3 %all-to-all-start.4 = ((bf16[4,192,704]{2,1,0:T(8,128)(2,1)}), bf16[4,192,704]{2,1,0:T(8,128)(2,1)}, u32[]{:S(2)}, u32[]{:S(2)}) async-start(bf16[4,192,704]{2,1,0:T(8,128)(2,1)} %broadcast_in_dim.17), calls=%async_computation.4 | async-start | bytes 2359296 | tf_op jit(solution)/shard_map/all_to_all | solution.py:14
  138.0 24.8 %all-to-all-start.8 = ((bf16[4,3,352,256]{3,2,1,0:T(8,128)(2,1)}), bf16[4,3,352,256]{3,2,1,0:T(8,128)(2,1)S(1)}, u32[]{:S(2)}, u32[]{:S(2)}) async-start(bf16[4,3,352,256]{3,2,1,0:T(8,128)(2,1)} %copy.34), calls=%async_computation.8 | async-start | bytes 4325376 | tf_op jit(solution)/shard_map/all_to_all | solution.py:14
  162.8 19.8 %all-to-all-start.5 = ((bf16[16,48,1024]{2,1,0:T(8,128)(2,1)}), bf16[16,48,1024]{2,1,0:T(8,128)(2,1)}, u32[]{:S(2)}, u32[]{:S(2)}) async-start(bf16[16,48,1024]{2,1,0:T(8,128)(2,1)} %bitcast.96), calls=%async_computation.5 | async-start | bytes 3145728 | tf_op jit(solution)/shard_map/all_to_all | solution.py:14
  168.9 33.0 %collective-permute-start.1 = (bf16[3,352,1024]{2,1,0:T(8,128)(2,1)}, bf16[3,352,1024]{2,1,0:T(8,128)(2,1)S(1)}, u32[]{:S(2)}, u32[]{:S(2)}) collective-permute-start(bf16[3,352,1024]{2,1,0:T(8,128)(2,1)} %bitcast.60), channel_id=1, source_target_pairs={{0,1},{1,0},{2,3},{3,2},{4,5},{5,4},{6,7},{7,6},{8,9},{9,8},{10,11... | collective-permute-start | bytes 6488072 | tf_op jit(solution)/shard_map/ppermute | solution.py:22
  194.8 20.6 %all-to-all-start.7 = ((bf16[16,48,1024]{2,1,0:T(8,128)(2,1)}), bf16[16,48,1024]{2,1,0:T(8,128)(2,1)}, u32[]{:S(2)}, u32[]{:S(2)}) async-start(bf16[16,48,1024]{2,1,0:T(8,128)(2,1)} %broadcast_in_dim.18), calls=%async_computation.7 | async-start | bytes 3145728 | tf_op jit(solution)/shard_map/all_to_all | solution.py:14
  202.1 2.0 copy-start.3
  264.6 18.7 %all-to-all-start.11 = ((bf16[16,192,256]{2,1,0:T(8,128)(2,1)}), bf16[16,192,256]{2,1,0:T(8,128)(2,1)S(1)}, u32[]{:S(2)}, u32[]{:S(2)}) async-start(bf16[16,192,256]{2,1,0:T(8,128)(2,1)} %bitcast.85), calls=%async_computation.11 | async-start | bytes 3145728 | tf_op jit(solution)/shard_map/all_to_all | solution.py:14
  283.3 65.7 %copy-start.1 = (bf16[1536,256]{1,0:T(8,128)(2,1)S(1)}, bf16[1536,256]{1,0:T(8,128)(2,1)}, u32[]{:S(2)}) copy-start(bf16[1536,256]{1,0:T(8,128)(2,1)} %param.6) | copy-start | bytes 2359300
  326.6 21.2 %collective-permute-start.2 = (bf16[768,256]{1,0:T(8,128)(2,1)S(1)}, bf16[768,256]{1,0:T(8,128)(2,1)S(1)}, u32[]{:S(2)}, u32[]{:S(2)}) collective-permute-start(bf16[768,256]{1,0:T(8,128)(2,1)S(1)} %bitcast.98), channel_id=1, source_target_pairs={{0,1},{1,0},{2,3},{3,2},{4,5},{5,4},{6,7},{7,6},{8,9},{9,8},{10,11... | collective-permute-start | bytes 1179656 | tf_op jit(solution)/shard_map/ppermute | solution.py:22
